TPU v7x, 32 devices: a whole 2x2x4 slice. The times are simulated.
32 devices in a mesh: kv: 8 (over z, x), tp: 4 (over y, core).
Axes of the slice: x: 2, y: 2, z: 4, core: 2. Of those that a mesh axis runs over, the one named last changes fastest.
Arguments:
- hidden: bfloat16 [128, 4, 2048], P(None, None, 'kv'), may hold values from -18 to 18
- norm_gain: float32 [2048], replicated, may hold values from 0.1 to 1.9
- w_query: bfloat16 [2048, 1024], P(None, 'tp'), may hold values from -0.125 to 0.125
- w_forget: bfloat16 [2048, 1024], P(None, 'tp'), may hold values from -0.125 to 0.125
- w_input: bfloat16 [2048, 1024], P(None, 'tp'), may hold values from -0.125 to 0.125
- w_outgate: bfloat16 [2048, 1024], P(None, 'tp'), may hold values from -0.125 to 0.125
- w_out: bfloat16 [1024, 2048], replicated, may hold values from -0.1875 to 0.1875
- floor: float32 [1024], P('tp'), may hold values from 0 to 0.95
- head_gain: float32 [128], replicated, may hold values from 0.1 to 1.9
- base_state: float32 [128, 8, 128, 128], P('kv', 'tp'), may hold values from -4 to 4
- prev_forget: bfloat16 [128, 4, 1024], P('kv', None, 'tp'), may hold values from -6 to 6
- prev_input: bfloat16 [128, 4, 1024], P('kv', None, 'tp'), may hold values from -6 to 6
- accepted: int32 [128], P('kv'), may hold values from 0 to 4
Outputs:
- mixed: bfloat16 [128, 4, 2048], P(None, None, 'kv')
- taken_state: float32 [128, 8, 128, 128], P('kv', 'tp')
All inputs are finite; a program needn't handle non-finite values.
Results may differ from a plain program's by a relative error of at most 0.014.
Values may be sent and summed in bfloat16 or wider, within the bound.
A program may use at most 64 MiB of HBM per device.

v0:
```python
import jax
import jax.numpy as jnp
from jax import lax
from jax.sharding import PartitionSpec as P

D = 2048
HEAD_DIM = 128
PROPS = 4


def shards(
    hidden,
    norm_gain,
    w_query,
    w_forget,
    w_input,
    w_outgate,
    w_out,
    floor,
    head_gain,
    base_state,
    prev_forget,
    prev_input,
    accepted,
):
    arrived = lax.all_to_all(hidden, "kv", split_axis=0, concat_axis=2, tiled=True)
    whole_vals = arrived.astype(jnp.float32)
    row_sums = jnp.sum(whole_vals * whole_vals, axis=2)
    normed = (whole_vals * lax.rsqrt(row_sums / D + 1e-06)[..., None] * norm_gain).astype(
        jnp.bfloat16
    )
    query_pre = jnp.dot(normed, w_query, preferred_element_type=jnp.float32).astype(jnp.bfloat16)
    forget_pre = jnp.dot(normed, w_forget, preferred_element_type=jnp.float32).astype(jnp.bfloat16)
    input_pre = jnp.dot(normed, w_input, preferred_element_type=jnp.float32).astype(jnp.bfloat16)
    gate_pre = jnp.dot(normed, w_outgate, preferred_element_type=jnp.float32).astype(jnp.bfloat16)
    seq_local = normed.shape[0]
    head_local = w_query.shape[1] // HEAD_DIM
    shape = (seq_local, PROPS, head_local, HEAD_DIM)
    query = jax.nn.silu(query_pre.astype(jnp.float32)).reshape(shape)
    forget = (floor + (1.0 - floor) * jax.nn.sigmoid(forget_pre.astype(jnp.float32))).reshape(shape)
    value = input_pre.astype(jnp.float32).reshape(shape)
    prev_f = (floor + (1.0 - floor) * jax.nn.sigmoid(prev_forget.astype(jnp.float32))).reshape(
        shape
    )
    prev_v = prev_input.astype(jnp.float32).reshape(shape)
    state = base_state
    for step in range(PROPS):
        live = (step < accepted)[:, None, None, None]
        moved = (
            prev_f[:, step][..., None] * state
            + (1.0 - prev_f[:, step])[..., None] * prev_v[:, step][:, :, None, :]
        )
        state = jnp.where(live, moved, state)
    taken_state = state
    outputs = []
    for step in range(PROPS):
        state = (
            forget[:, step][..., None] * state
            + (1.0 - forget[:, step])[..., None] * value[:, step][:, :, None, :]
        )
        outputs.append(
            jnp.einsum("bhk,bhkv->bhv", query[:, step], state, precision=lax.Precision.HIGHEST)
        )
    result = jnp.stack(outputs, axis=1)
    scaled = (
        result * lax.rsqrt(jnp.mean(result * result, axis=-1, keepdims=True) + 1e-05) * head_gain
    )
    gated = scaled * jax.nn.silu(gate_pre.astype(jnp.float32)).reshape(shape)
    mixed_heads = gated.reshape(seq_local, PROPS, head_local * HEAD_DIM).astype(jnp.bfloat16)
    own_rows = mixed_heads.shape[2]
    w_rows = lax.dynamic_slice_in_dim(w_out, lax.axis_index("tp") * own_rows, own_rows, 0)
    partial_value = jnp.dot(mixed_heads, w_rows, preferred_element_type=jnp.float32)
    finished = lax.psum(partial_value, "tp").astype(jnp.bfloat16)
    mixed = lax.all_to_all(finished, "kv", split_axis=2, concat_axis=0, tiled=True)
    return (mixed, taken_state)


def solution(mesh):
    placed = (
        P(None, None, "kv"),
        P(),
        P(None, "tp"),
        P(None, "tp"),
        P(None, "tp"),
        P(None, "tp"),
        P(),
        P("tp"),
        P(),
        P("kv", "tp", None, None),
        P("kv", None, "tp"),
        P("kv", None, "tp"),
        P("kv"),
    )
    return jax.shard_map(
        shards,
        mesh=mesh,
        in_specs=placed,
        out_specs=(P(None, None, "kv"), P("kv", "tp", None, None)),
        check_vma=False,
    )
```

profile of v0, /device:TPU:0, one launch (start us, length us, event | category | flops | bytes accessed | tf_op | source)
XLA Modules:
  0.0 96.0 jit_solution(18002514994027775703)
XLA Ops:
  0.6 7.4 %all-to-all-start = ((bf16[128,4,256]{2,1,0:T(4,128)(2,1)}), bf16[128,4,256]{2,1,0:T(4,128)(2,1)S(1)}, u32[]{:S(2)}, u32[]{:S(2)}) async-start(bf16[128,4,256]{2,1,0:T(4,128)(2,1)} %param.13), calls=%async_computation | async-start | bytes 524288 | tf_op jit(solution)/shard_map/all_to_all | solution.py:26
  9.3 0.8 multiply_add_fusion.9
  10.2 1.2 %broadcast_bitcast_fusion = f32[256]{0:T(256)} fusion(f32[128]{0:T(128)} %param.21), kind=kLoop, calls=%fused_computation.82 | loop fusion | bytes 1536 | tf_op jit(solution)/shard_map/mul | solution.py:66
  11.5 1.3 %broadcast_compare_fusion.3 = (pred[16]{0:T(512)(128)(4,1)}, pred[16]{0:T(512)(128)(4,1)}, pred[16]{0:T(512)(128)(4,1)}, pred[16]{0:T(512)(128)(4,1)}) fusion(s32[16]{0:T(128)} %param.25), kind=kLoop, calls=%fused_computation.88 | loop fusion | flops 64 | bytes 128 | tf_op jit(solution)/shard_map/gt | solution.py:48
  12.7 0.8 reshape.130
  14.1 7.1 %add_select_fusion = f32[16,2,128,128]{3,2,1,0:T(8,128)S(1)} fusion(f32[16,2,128,128]{3,2,1,0:T(8,128)} %param.22, f32[16,2,128]{2,1,0:T(2,128)} %get-tuple-element.29, f32[16,2,128]{2,1,0:T(2,128)S(1)} %get-tuple-element.25, f32[16,2,128]{2,1,0:T(2,128)} %get-tuple-element.27, f32[16,2,128]{2,1,0:T(2,128)S(1)} %get-tuple-element.24, ...), kind=kLoop, calls=%fused_computation.7 | loop fusion | flops 8388608 | bytes 4390976 | tf_op jit(solution)/shard_map/jit(_where)/select_n | solution.py:53
  21.7 1.1 %copy.38 = f32[16,4,8,256]{3,2,0,1:T(8,128)} copy(f32[16,4,8,256]{3,1,0,2:T(4,128)S(1)} %bitcast.141) | data formatting | bytes 1048576 | tf_op jit(solution)/shard_map/convert_element_type | solution.py:27
  22.8 1.9 %reshape.128 = f32[16,4,2048]{2,0,1:T(8,128)} reshape(f32[16,4,8,256]{3,2,0,1:T(8,128)} %copy.38) | data formatting | bytes 1048576 | tf_op jit(solution)/shard_map/convert_element_type | solution.py:27
  24.8 1.2 %multiply_convert_fusion = bf16[16,4,2048]{2,0,1:T(8,128)(2,1)S(1)} fusion(f32[16,4,2048]{2,0,1:T(8,128)} %reshape.128, f32[2048]{0:T(1024)S(1)} %copy-done.5, f32[16,4]{0,1:T(4,128)S(1)} %add_rsqrt_fusion.1), kind=kLoop, calls=%fused_computation.43 | loop fusion | flops 393216 | bytes 794880 | tf_op jit(solution)/shard_map/convert_element_type | solution.py:29
  25.9 1.5 %fusion.14 = f32[16,4,256]{2,0,1:T(8,128)S(1)} fusion(bf16[16,4,2048]{2,0,1:T(8,128)(2,1)S(1)} %multiply_convert_fusion, bf16[2048,256]{1,0:T(8,128)(2,1)} %param.16, f32[256]{0:T(256)S(1)} %copy-done.4, f32[256]{0:T(256)S(1)} %copy-done.2), kind=kOutput, calls=%fused_computation.21 | convolution fusion | flops 67223552 | bytes 1378304 | tf_op jit(solution)/shard_map/dot_general | solution.py:33
  27.5 1.5 %fusion.7 = f32[16,4,256]{2,0,1:T(8,128)S(1)} fusion(bf16[16,4,2048]{2,0,1:T(8,128)(2,1)S(1)} %multiply_convert_fusion, bf16[2048,256]{1,0:T(8,128)(2,1)} %param.17), kind=kOutput, calls=%fused_computation.13 | convolution fusion | flops 67141632 | bytes 1376256 | tf_op jit(solution)/shard_map/dot_general | solution.py:34
  29.7 2.2 %divide_multiply_fusion = f32[16,4,256]{2,0,1:T(8,128)} fusion(bf16[16,4,2048]{2,0,1:T(8,128)(2,1)S(1)} %multiply_convert_fusion, bf16[2048,256]{1,0:T(8,128)(2,1)} %param.15), kind=kOutput, calls=%fused_computation.53 | convolution fusion | flops 67207168 | bytes 1376256 | tf_op jit(solution)/shard_map/dot_general | solution.py:32
  31.9 0.9 reshape.121
  33.6 2.8 %fusion.4 = f32[16,2,1,128]{3,2,1,0:T(1,128)S(1)} fusion(f32[16,2,128,1]{2,3,1,0:T(1,128)S(1)} %bitcast.146, f32[16,2,128,128]{3,2,1,0:T(8,128)S(1)} %add_select_fusion, f32[16,2,128]{2,1,0:T(2,128)S(1)} %get-tuple-element.14, f32[16,2,128]{2,1,0:T(2,128)S(1)} %get-tuple-element.10, f32[16,2,128]{2,1,0:T(2,128)S(1)} %get-tuple-element.37), kind=kOutput, calls=%fused_computation.8 | convolution fusion | flops 7864320 | bytes 2179072 | tf_op jit(solution)/shard_map/bhk,bhkv->bhv/dot_general | solution.py:62
  36.4 4.3 %fusion.35 = f32[16,2,1,128]{3,2,1,0:T(1,128)S(1)} fusion(f32[16,2,128,1]{2,3,1,0:T(1,128)S(1)} %bitcast.155, f32[16,2,128,128]{3,2,1,0:T(8,128)S(1)} %add_select_fusion, f32[16,2,128]{2,1,0:T(2,128)S(1)} %get-tuple-element.17, f32[16,2,128]{2,1,0:T(2,128)S(1)} %get-tuple-element.13, f32[16,2,128]{2,1,0:T(2,128)S(1)} %get-tuple-element.34, ...), kind=kOutput, calls=%fused_computation.45 | convolution fusion | flops 9437184 | bytes 2228224 | tf_op jit(solution)/shard_map/bhk,bhkv->bhv/dot_general | solution.py:62
  40.7 6.1 %fusion.5 = f32[16,2,1,128]{3,2,1,0:T(1,128)S(1)} fusion(f32[16,2,128,1]{2,3,1,0:T(1,128)S(1)} %bitcast.154, f32[16,2,128]{2,1,0:T(2,128)S(1)} %get-tuple-element.16, f32[16,2,128]{2,1,0:T(2,128)S(1)} %get-tuple-element.12, f32[16,2,128]{2,1,0:T(2,128)S(1)} %get-tuple-element.35, f32[16,2,128,128]{3,2,1,0:T(8,128)S(1)} %add_select_fusion, ...), kind=kOutput, calls=%fused_computation.9 | convolution fusion | flops 11010048 | bytes 2277376 | tf_op jit(solution)/shard_map/bhk,bhkv->bhv/dot_general | solution.py:62
  46.8 7.2 %fusion = f32[16,2,1,128]{3,2,1,0:T(1,128)S(1)} fusion(f32[16,2,128,1]{2,3,1,0:T(1,128)S(1)} %bitcast.153, f32[16,2,128]{2,1,0:T(2,128)S(1)} %get-tuple-element.15, f32[16,2,128]{2,1,0:T(2,128)S(1)} %get-tuple-element.11, f32[16,2,128]{2,1,0:T(2,128)S(1)} %get-tuple-element.36, f32[16,2,128]{2,1,0:T(2,128)S(1)} %get-tuple-element.16, ...), kind=kOutput, calls=%fused_computation | convolution fusion | flops 12582912 | bytes 2326528 | tf_op jit(solution)/shard_map/bhk,bhkv->bhv/dot_general | solution.py:62
  54.4 2.0 %fusion.16 = f32[16,4,2048]{2,0,1:T(8,128)S(1)} fusion(bf16[1024,2048]{1,0:T(8,128)(2,1)} %param.19, s32[]{:T(128)S(6)} %select_n.20, f32[16,4,256]{2,0,1:T(8,128)S(1)} %mul.344, f32[16,1,256]{2,0,1:T(8,128)S(1)} %stack.28, f32[16,1,256]{2,0,1:T(8,128)S(1)} %stack.27, f32[16,1,256]{2,0,1:T(8,128)S(1)} %stack.26, f32[16,1,256]{2,0,1:T(8,128)S(1)} %stack.25, ...), kind=kOutput, calls=%fused_computation.24 | convolution fusion | flops 134430720 | bytes 3015684 | tf_op jit(solution)/shard_map/dot_general | solution.py:72
  56.5 16.6 %all-reduce.1 = bf16[16,4,2048]{2,0,1:T(8,128)(2,1)S(1)} all-reduce(f32[16,4,2048]{2,0,1:T(8,128)S(1)} %fusion.16), channel_id=1, replica_groups=mesh['kv'=8,'tp'=4] {'tp'}, use_global_device_ids=true, to_apply=%region_3.4 | all-reduce | flops 131072 | bytes 786432 | tf_op jit(solution)/shard_map/psum | solution.py:73
  73.1 1.4 %copy.45 = bf16[16,4,2048]{0,1,2:T(4,128)(2,1)S(1)} copy(bf16[16,4,2048]{2,0,1:T(8,128)(2,1)S(1)} %all-reduce.1) | data formatting | bytes 524288 | tf_op jit(solution)/shard_map/convert_element_type | solution.py:73
  74.5 2.2 %reshape.148 = bf16[8,2,8192]{2,1,0:T(2,128)(2,1)S(1)} reshape(bf16[2048,4,16]{2,1,0:T(4,128)(2,1)S(1)} %bitcast.139) | data formatting | bytes 524288
  76.7 14.9 %all_to_all.27 = bf16[8,2,8192]{2,1,0:T(2,128)(2,1)} all-to-all(bf16[8,2,8192]{2,1,0:T(2,128)(2,1)S(1)} %reshape.148), channel_id=1, replica_groups=mesh['kv'=8,'tp'=4] {'kv'}, dimensions={0} | all-to-all | bytes 524288 | tf_op jit(solution)/shard_map/all_to_all | solution.py:74
  91.5 2.4 %reshape.149 = bf16[2048,4,16]{2,1,0:T(4,128)(2,1)S(1)} reshape(bf16[8,2,8192]{2,1,0:T(2,128)(2,1)} %all_to_all.27) | data formatting | bytes 524288
  94.0 2.0 %copy.46 = bf16[8,16,4,256]{3,2,1,0:T(4,128)(2,1)} copy(bf16[8,16,4,256]{1,2,3,0:T(4,128)(2,1)S(1)} %bitcast.140) | data formatting | bytes 524288 | tf_op jit(solution)/shard_map/all_to_all | solution.py:74
  (38 shorter events, 4.3 us)
Async XLA Ops:
  0.6 53.8 %copy-start = (bf16[2048,256]{1,0:T(8,128)(2,1)S(1)}, bf16[2048,256]{1,0:T(8,128)(2,1)}, u32[]{:S(2)}) copy-start(bf16[2048,256]{1,0:T(8,128)(2,1)} %param.18) | copy-start | bytes 3145732
  0.6 20.7 %all-to-all-start = ((bf16[128,4,256]{2,1,0:T(4,128)(2,1)}), bf16[128,4,256]{2,1,0:T(4,128)(2,1)S(1)}, u32[]{:S(2)}, u32[]{:S(2)}) async-start(bf16[128,4,256]{2,1,0:T(4,128)(2,1)} %param.13), calls=%async_computation | async-start | bytes 524288 | tf_op jit(solution)/shard_map/all_to_all | solution.py:26
  8.8 0.6 copy-start.3
  21.3 25.5 %copy-start.1 = (f32[16,2,128,128]{3,2,1,0:T(8,128)}, f32[16,2,128,128]{3,2,1,0:T(8,128)S(1)}, u32[]{:S(2)}) copy-start(f32[16,2,128,128]{3,2,1,0:T(8,128)S(1)} %add_select_fusion) | copy-start | bytes 6291460
  21.3 3.5 %copy-start.5 = (f32[2048]{0:T(1024)S(1)}, f32[2048]{0:T(1024)}, u32[]{:S(2)}) copy-start(f32[2048]{0:T(1024)} %param.14) | copy-start | bytes 24580
  21.3 4.6 %copy-start.2 = (f32[256]{0:T(256)S(1)}, f32[256]{0:T(256)}, u32[]{:S(2)}) copy-start(f32[256]{0:T(256)} %param.20) | copy-start | bytes 3076
  21.3 4.6 %copy-start.4 = (f32[256]{0:T(256)S(1)}, f32[256]{0:T(256)}, u32[]{:S(2)}) copy-start(f32[256]{0:T(256)} %copy-done.3) | copy-start | bytes 3076
  46.8 7.7 %copy-start.6 = (f32[256]{0:T(256)S(1)}, f32[256]{0:T(256)}, u32[]{:S(2)}) copy-start(f32[256]{0:T(256)} %broadcast_bitcast_fusion) | copy-start | bytes 3076
where the time goes:
time: 96.9 us; the launch traced here: 96 us
  blocking collectives  31.5 us (33%)
  matrix products  27.6 us (28%)
  local copies, waits for them, and re-layouts  17 us (18%)
  other arithmetic  11.5 us (12%)
  starting transfers between devices  7.42 us (8%)
    dot_general x4, matrix products, shards(): jnp.einsum('bhk,bhkv->bhv', query[:, step], state, precision=lax.Precisio...  20.3 us
    psum x1, blocking collectives, shards(): finished = lax.psum(partial_value, 'tp').astype(jnp.bfloat16)  16.6 us
    all_to_all x1, blocking collectives, shards(): lax.all_to_all(finished, 'kv', split_axis=2, concat_axis=0, tiled=True)  14.9 us
    all_to_all x1, starting transfers between devices, shards(): lax.all_to_all(hidden, 'kv', split_axis=0, concat_axis=2, tiled=True)  7.42 us
    select_n x1, other arithmetic, shards(): state = jnp.where(live, moved, state)  7.13 us
    unnamed x17, local copies, waits for them, and re-layouts  5.27 us
    convert_element_type x2, local copies, waits for them, and re-layouts, shards(): whole_vals = arrived.astype(jnp.float32)  3.03 us
    dot_general x1, matrix products, shards(): jnp.dot(normed, w_query, preferred_element_type=jnp.float32)  2.17 us
  transfers between devices with their start and end apart: 1, of which 0 were waited for; matrix products, arithmetic and copies ran while one was open for 13% of the time, Pallas kernels for 0%

commit v1 on v0

--- a/solution.py
+++ b/solution.py
@@ -71,7 +71,10 @@
     w_rows = lax.dynamic_slice_in_dim(w_out, lax.axis_index("tp") * own_rows, own_rows, 0)
     partial_value = jnp.dot(mixed_heads, w_rows, preferred_element_type=jnp.float32)
     finished = lax.psum(partial_value, "tp").astype(jnp.bfloat16)
-    mixed = lax.all_to_all(finished, "kv", split_axis=2, concat_axis=0, tiled=True)
+    mixed = jnp.concatenate(
+        lax.all_to_all(jnp.stack(jnp.split(finished, lax.axis_size("kv"), axis=2)), "kv", 0, 0),
+        axis=0,
+    )
     return (mixed, taken_state)
 
 

time: 96.9 us -> 89.9 us (0.928)
  local copies, waits for them, and re-layouts: 17 us -> 10 us
    unnamed x17 -> x23, local copies, waits for them, and re-layouts: 5.27 us -> 1.64 us
    all_to_all x1, local copies, waits for them, and re-layouts: 2.02 us -> 0.02 us  [shards(): lax.all_to_all(jnp.stack(jnp.split(finished, lax.axis_size('kv'), axis=2)...]
    convert_element_type x1 -> x0, local copies, waits for them, and re-layouts: 1.36 us -> none  [shards(): finished = lax.psum(partial_value, 'tp').astype(jnp.bfloat16)]
  transfers between devices with their start and end apart: 1 -> 1, of which waited for: 0 -> 0; matrix products, arithmetic and copies ran while one was open for 13% -> 14% of each run, Pallas kernels for 0% -> 0%
where the time goes in v1:
time: 89.9 us; the launch traced here: 88.9 us
  blocking collectives  31.4 us (35%)
  matrix products  27.6 us (31%)
  other arithmetic  11.5 us (13%)
  local copies, waits for them, and re-layouts  10 us (11%)
  starting transfers between devices  7.42 us (8%)
  between operations  0.98 us (1%)
    dot_general x4, matrix products, shards(): jnp.einsum('bhk,bhkv->bhv', query[:, step], state, precision=lax.Precisio...  20.3 us
    psum x1, blocking collectives, shards(): finished = lax.psum(partial_value, 'tp').astype(jnp.bfloat16)  16.6 us
    all_to_all x1, blocking collectives, shards(): lax.all_to_all(jnp.stack(jnp.split(finished, lax.axis_size('kv'), axis=2)...  14.7 us
    all_to_all x1, starting transfers between devices, shards(): lax.all_to_all(hidden, 'kv', split_axis=0, concat_axis=2, tiled=True)  7.42 us
    select_n x1, other arithmetic, shards(): state = jnp.where(live, moved, state)  7.13 us
    convert_element_type x2, local copies, waits for them, and re-layouts, shards(): whole_vals = arrived.astype(jnp.float32)  3.03 us
    dot_general x1, matrix products, shards(): jnp.dot(normed, w_query, preferred_element_type=jnp.float32)  2.17 us
    dot_general x1, matrix products, shards(): jnp.dot(mixed_heads, w_rows, preferred_element_type=jnp.float32)  2.04 us
  transfers between devices with their start and end apart: 1, of which 0 were waited for; matrix products, arithmetic and copies ran while one was open for 14% of the time, Pallas kernels for 0%

profile of v1, /device:TPU:0, one launch (start us, length us, event | category | flops | bytes accessed | tf_op | source)
XLA Modules:
  0.0 88.9 jit_solution(12442321354526438328)
XLA Ops:
  0.6 7.4 %all-to-all-start = ((bf16[128,4,256]{2,1,0:T(4,128)(2,1)}), bf16[128,4,256]{2,1,0:T(4,128)(2,1)S(1)}, u32[]{:S(2)}, u32[]{:S(2)}) async-start(bf16[128,4,256]{2,1,0:T(4,128)(2,1)} %param.13), calls=%async_computation | async-start | bytes 524288 | tf_op jit(solution)/shard_map/all_to_all | solution.py:26
  8.1 0.7 broadcast_subtract_fusion.8
  9.3 0.8 multiply_add_fusion.9
  10.2 1.2 %broadcast_bitcast_fusion = f32[256]{0:T(256)} fusion(f32[128]{0:T(128)} %param.21), kind=kLoop, calls=%fused_computation.98 | loop fusion | bytes 1536 | tf_op jit(solution)/shard_map/mul | solution.py:66
  11.5 1.3 %broadcast_compare_fusion.3 = (pred[16]{0:T(512)(128)(4,1)}, pred[16]{0:T(512)(128)(4,1)}, pred[16]{0:T(512)(128)(4,1)}, pred[16]{0:T(512)(128)(4,1)}) fusion(s32[16]{0:T(128)} %param.25), kind=kLoop, calls=%fused_computation.104 | loop fusion | flops 64 | bytes 128 | tf_op jit(solution)/shard_map/gt | solution.py:48
  12.7 0.8 reshape.134
  14.1 7.1 %add_select_fusion = f32[16,2,128,128]{3,2,1,0:T(8,128)S(1)} fusion(f32[16,2,128,128]{3,2,1,0:T(8,128)} %param.22, f32[16,2,128]{2,1,0:T(2,128)} %get-tuple-element.35, f32[16,2,128]{2,1,0:T(2,128)S(1)} %get-tuple-element.31, f32[16,2,128]{2,1,0:T(2,128)} %get-tuple-element.33, f32[16,2,128]{2,1,0:T(2,128)S(1)} %get-tuple-element.30, ...), kind=kLoop, calls=%fused_computation.7 | loop fusion | flops 8388608 | bytes 4390976 | tf_op jit(solution)/shard_map/jit(_where)/select_n | solution.py:53
  21.7 1.1 %copy.37 = f32[16,4,8,256]{3,2,0,1:T(8,128)} copy(f32[16,4,8,256]{3,1,0,2:T(4,128)S(1)} %bitcast.166) | data formatting | bytes 1048576 | tf_op jit(solution)/shard_map/convert_element_type | solution.py:27
  22.8 1.9 %reshape.132 = f32[16,4,2048]{2,0,1:T(8,128)} reshape(f32[16,4,8,256]{3,2,0,1:T(8,128)} %copy.37) | data formatting | bytes 1048576 | tf_op jit(solution)/shard_map/convert_element_type | solution.py:27
  24.8 1.2 %multiply_convert_fusion = bf16[16,4,2048]{2,0,1:T(8,128)(2,1)S(1)} fusion(f32[16,4,2048]{2,0,1:T(8,128)} %reshape.132, f32[2048]{0:T(1024)S(1)} %copy-done.5, f32[16,4]{0,1:T(4,128)S(1)} %add_rsqrt_fusion.1), kind=kLoop, calls=%fused_computation.43 | loop fusion | flops 393216 | bytes 794880 | tf_op jit(solution)/shard_map/convert_element_type | solution.py:29
  25.9 1.5 %fusion.14 = f32[16,4,256]{2,0,1:T(8,128)S(1)} fusion(bf16[16,4,2048]{2,0,1:T(8,128)(2,1)S(1)} %multiply_convert_fusion, bf16[2048,256]{1,0:T(8,128)(2,1)} %param.16, f32[256]{0:T(256)S(1)} %copy-done.4, f32[256]{0:T(256)S(1)} %copy-done.2), kind=kOutput, calls=%fused_computation.21 | convolution fusion | flops 67223552 | bytes 1378304 | tf_op jit(solution)/shard_map/dot_general | solution.py:33
  27.5 1.5 %fusion.7 = f32[16,4,256]{2,0,1:T(8,128)S(1)} fusion(bf16[16,4,2048]{2,0,1:T(8,128)(2,1)S(1)} %multiply_convert_fusion, bf16[2048,256]{1,0:T(8,128)(2,1)} %param.17), kind=kOutput, calls=%fused_computation.13 | convolution fusion | flops 67141632 | bytes 1376256 | tf_op jit(solution)/shard_map/dot_general | solution.py:34
  29.1 0.7 reshape.136
  29.7 2.2 %divide_multiply_fusion = f32[16,4,256]{2,0,1:T(8,128)} fusion(bf16[16,4,2048]{2,0,1:T(8,128)(2,1)S(1)} %multiply_convert_fusion, bf16[2048,256]{1,0:T(8,128)(2,1)} %param.15), kind=kOutput, calls=%fused_computation.53 | convolution fusion | flops 67207168 | bytes 1376256 | tf_op jit(solution)/shard_map/dot_general | solution.py:32
  31.9 0.9 reshape.124
  32.8 0.8 slice_bitcast_fusion.14
  33.6 2.8 %fusion.4 = f32[16,2,1,128]{3,2,1,0:T(1,128)S(1)} fusion(f32[16,2,128,1]{2,3,1,0:T(1,128)S(1)} %bitcast.171, f32[16,2,128,128]{3,2,1,0:T(8,128)S(1)} %add_select_fusion, f32[16,2,128]{2,1,0:T(2,128)S(1)} %get-tuple-element.20, f32[16,2,128]{2,1,0:T(2,128)S(1)} %get-tuple-element.16, f32[16,2,128]{2,1,0:T(2,128)S(1)} %get-tuple-element.43), kind=kOutput, calls=%fused_computation.8 | convolution fusion | flops 7864320 | bytes 2179072 | tf_op jit(solution)/shard_map/bhk,bhkv->bhv/dot_general | solution.py:62
  36.4 4.3 %fusion.35 = f32[16,2,1,128]{3,2,1,0:T(1,128)S(1)} fusion(f32[16,2,128,1]{2,3,1,0:T(1,128)S(1)} %bitcast.180, f32[16,2,128,128]{3,2,1,0:T(8,128)S(1)} %add_select_fusion, f32[16,2,128]{2,1,0:T(2,128)S(1)} %get-tuple-element.23, f32[16,2,128]{2,1,0:T(2,128)S(1)} %get-tuple-element.19, f32[16,2,128]{2,1,0:T(2,128)S(1)} %get-tuple-element.40, ...), kind=kOutput, calls=%fused_computation.45 | convolution fusion | flops 9437184 | bytes 2228224 | tf_op jit(solution)/shard_map/bhk,bhkv->bhv/dot_general | solution.py:62
  40.7 6.1 %fusion.5 = f32[16,2,1,128]{3,2,1,0:T(1,128)S(1)} fusion(f32[16,2,128,1]{2,3,1,0:T(1,128)S(1)} %bitcast.179, f32[16,2,128]{2,1,0:T(2,128)S(1)} %get-tuple-element.22, f32[16,2,128]{2,1,0:T(2,128)S(1)} %get-tuple-element.18, f32[16,2,128]{2,1,0:T(2,128)S(1)} %get-tuple-element.41, f32[16,2,128,128]{3,2,1,0:T(8,128)S(1)} %add_select_fusion, ...), kind=kOutput, calls=%fused_computation.9 | convolution fusion | flops 11010048 | bytes 2277376 | tf_op jit(solution)/shard_map/bhk,bhkv->bhv/dot_general | solution.py:62
  46.8 7.2 %fusion = f32[16,2,1,128]{3,2,1,0:T(1,128)S(1)} fusion(f32[16,2,128,1]{2,3,1,0:T(1,128)S(1)} %bitcast.178, f32[16,2,128]{2,1,0:T(2,128)S(1)} %get-tuple-element.21, f32[16,2,128]{2,1,0:T(2,128)S(1)} %get-tuple-element.17, f32[16,2,128]{2,1,0:T(2,128)S(1)} %get-tuple-element.42, f32[16,2,128]{2,1,0:T(2,128)S(1)} %get-tuple-element.22, ...), kind=kOutput, calls=%fused_computation | convolution fusion | flops 12582912 | bytes 2326528 | tf_op jit(solution)/shard_map/bhk,bhkv->bhv/dot_general | solution.py:62
  54.4 2.0 %fusion.16 = f32[16,4,2048]{2,0,1:T(8,128)S(1)} fusion(bf16[1024,2048]{1,0:T(8,128)(2,1)} %param.19, s32[]{:T(128)S(6)} %select_n.20, f32[16,4,256]{2,0,1:T(8,128)S(1)} %mul.344, f32[16,1,256]{2,0,1:T(8,128)S(1)} %stack.55, f32[16,1,256]{2,0,1:T(8,128)S(1)} %stack.54, f32[16,1,256]{2,0,1:T(8,128)S(1)} %stack.53, f32[16,1,256]{2,0,1:T(8,128)S(1)} %stack.52, ...), kind=kOutput, calls=%fused_computation.24 | convolution fusion | flops 134430720 | bytes 3015684 | tf_op jit(solution)/shard_map/dot_general | solution.py:72
  56.5 16.6 %all-reduce.1 = bf16[16,4,2048]{2,0,1:T(8,128)(2,1)S(1)} all-reduce(f32[16,4,2048]{2,0,1:T(8,128)S(1)} %fusion.16), channel_id=1, replica_groups=mesh['kv'=8,'tp'=4] {'tp'}, use_global_device_ids=true, to_apply=%region_3.4 | all-reduce | flops 131072 | bytes 786432 | tf_op jit(solution)/shard_map/psum | solution.py:73
  73.3 14.7 %all_to_all.14 = bf16[8,16,4,256]{3,1,2,0:T(8,128)(2,1)S(1)} all-to-all(bf16[8,16,4,256]{3,1,2,0:T(8,128)(2,1)S(1)} %fusion.46), channel_id=1, replica_groups=mesh['kv'=8,'tp'=4] {'kv'}, dimensions={0} | all-to-all | bytes 524288 | tf_op jit(solution)/shard_map/all_to_all | solution.py:75
  88.0 0.9 %copy.45 = bf16[128,4,256]{2,1,0:T(4,128)(2,1)} copy(bf16[128,4,256]{2,0,1:T(8,128)(2,1)S(1)} %bitcast.167) | data formatting | bytes 524288
  (44 shorter events, 2.3 us)
Async XLA Ops:
  0.6 53.8 %copy-start = (bf16[2048,256]{1,0:T(8,128)(2,1)S(1)}, bf16[2048,256]{1,0:T(8,128)(2,1)}, u32[]{:S(2)}) copy-start(bf16[2048,256]{1,0:T(8,128)(2,1)} %param.18) | copy-start | bytes 3145732
  0.6 20.7 %all-to-all-start = ((bf16[128,4,256]{2,1,0:T(4,128)(2,1)}), bf16[128,4,256]{2,1,0:T(4,128)(2,1)S(1)}, u32[]{:S(2)}, u32[]{:S(2)}) async-start(bf16[128,4,256]{2,1,0:T(4,128)(2,1)} %param.13), calls=%async_computation | async-start | bytes 524288 | tf_op jit(solution)/shard_map/all_to_all | solution.py:26
  8.8 0.6 copy-start.3
  21.3 25.5 %copy-start.1 = (f32[16,2,128,128]{3,2,1,0:T(8,128)}, f32[16,2,128,128]{3,2,1,0:T(8,128)S(1)}, u32[]{:S(2)}) copy-start(f32[16,2,128,128]{3,2,1,0:T(8,128)S(1)} %add_select_fusion) | copy-start | bytes 6291460
  21.3 3.5 %copy-start.5 = (f32[2048]{0:T(1024)S(1)}, f32[2048]{0:T(1024)}, u32[]{:S(2)}) copy-start(f32[2048]{0:T(1024)} %param.14) | copy-start | bytes 24580
  21.3 4.6 %copy-start.2 = (f32[256]{0:T(256)S(1)}, f32[256]{0:T(256)}, u32[]{:S(2)}) copy-start(f32[256]{0:T(256)} %param.20) | copy-start | bytes 3076
  21.3 4.6 %copy-start.4 = (f32[256]{0:T(256)S(1)}, f32[256]{0:T(256)}, u32[]{:S(2)}) copy-start(f32[256]{0:T(256)} %copy-done.3) | copy-start | bytes 3076
  46.8 7.7 %copy-start.6 = (f32[256]{0:T(256)S(1)}, f32[256]{0:T(256)}, u32[]{:S(2)}) copy-start(f32[256]{0:T(256)} %broadcast_bitcast_fusion) | copy-start | bytes 3076
